TPU v7x, 32 devices: a whole 2x2x4 slice. The times are simulated.
32 devices in a mesh: ep: 8 (over z, y), tp: 4 (over x, core).
Axes of the slice: x: 2, y: 2, z: 4, core: 2. Of those that a mesh axis runs over, the one named last changes fastest.
Arguments:
- tokens: bfloat16 [2048, 2048], P('ep', 'tp'), may hold values from -400 to 400
- expert_ids: int32 [2048, 2], P('ep'), may hold values from 0 to 7, all different within a row; in each aligned block of 256 rows (0 to 255, 256 to 511, ...) at most 80 rows name the same one
- route_weights: float32 [2048, 2], P('ep'), may hold values from 0.1 to 1
- pre_gain: float32 [2048], P('tp'), may hold values from 0.1 to 1.9
- post_gain: float32 [2048], P('tp'), may hold values from 0.1 to 1.9
- gate_weight: bfloat16 [8, 2048, 4096], P('ep', None, 'tp'), may hold values from -0.125 to 0.125
- up_weight: bfloat16 [8, 2048, 4096], P('ep', None, 'tp'), may hold values from -0.125 to 0.125
- down_weight: bfloat16 [8, 4096, 2048], P('ep', None, 'tp'), may hold values from -0.71875 to 0.71875
Outputs:
- layer_out: bfloat16 [2048, 2048], P('ep', 'tp')
Inputs may be any that keep to these rules, and one draw needn't show every extreme that they name: `expert_ids`: the 2 experts of a token are distinct. Within the rows of one device along ep, no expert is named more than 80 times, a bound that some block reaches.
All inputs are finite; a program needn't handle non-finite values.
Results may differ from a plain program's by a relative error of at most 0.007.
Values may be sent and summed in bfloat16 or wider, within the bound.
A program may use at most 64 MiB of HBM per device.

v0:
```python
import jax
import jax.numpy as jnp
from jax import lax
from jax.sharding import PartitionSpec as P

epsilon = 1e-06


def on_device(
    tokens, expert_ids, route_weights, pre_gain, post_gain, gate_weight, up_weight, down_weight
):
    tok_rows, width_part = tokens.shape
    width_full = width_part * lax.axis_size("tp")
    ep_count = lax.axis_size("ep")
    local_count = gate_weight.shape[0]
    experts_all = local_count * ep_count
    top_count = expert_ids.shape[1]
    capacity = max(2, tok_rows * top_count * 5 // (4 * experts_all))
    slot_total = experts_all * capacity
    tok_float = tokens.astype(jnp.float32)
    square_sum = lax.psum(jnp.sum(tok_float * tok_float, axis=1), "tp")
    inv_scale = lax.rsqrt(square_sum / width_full + epsilon)
    normed = (tok_float * inv_scale[:, None] * pre_gain[None, :]).astype(jnp.bfloat16)
    flat_ids = expert_ids.reshape(-1)
    onehot = (flat_ids[:, None] == jnp.arange(experts_all, dtype=jnp.int32)[None, :]).astype(
        jnp.int32
    )
    slot = jnp.sum((jnp.cumsum(onehot, axis=0) - 1) * onehot, axis=1)
    target = (flat_ids * capacity + slot).reshape(tok_rows, top_count)
    slot_index = jnp.arange(slot_total, dtype=jnp.int32)
    pick_map = (jnp.transpose(target).reshape(-1)[:, None] == slot_index[None, :]).astype(
        jnp.bfloat16
    )
    dispatch_map = jnp.sum(pick_map.reshape(top_count, tok_rows, slot_total), axis=0)
    outgoing = jnp.dot(
        jnp.transpose(dispatch_map), normed, preferred_element_type=jnp.float32
    ).astype(jnp.bfloat16)
    outgoing = outgoing.reshape(ep_count, local_count, capacity, width_part)
    arrived = lax.all_to_all(outgoing, "ep", split_axis=0, concat_axis=2, tiled=True)
    arrived = arrived.reshape(local_count, ep_count * capacity, width_part)
    row_total = ep_count * capacity
    features = lax.all_gather(arrived, "tp", axis=2, tiled=True)
    gate = jnp.einsum("erd,edh->erh", features, gate_weight, preferred_element_type=jnp.float32)
    upper = jnp.einsum("erd,edh->erh", features, up_weight, preferred_element_type=jnp.float32)
    hidden = (jax.nn.silu(gate) * upper).astype(jnp.bfloat16)
    hidden_whole = lax.all_gather(hidden, "tp", axis=2, tiled=True)
    result = jnp.einsum(
        "erh,ehd->erd", hidden_whole, down_weight, preferred_element_type=jnp.float32
    )
    expert_out = result.astype(jnp.bfloat16).reshape(1, local_count, row_total, width_part)
    returned = lax.all_to_all(expert_out, "ep", split_axis=2, concat_axis=0, tiled=True)
    returned = returned.reshape(slot_total, width_part)
    picked = jnp.dot(pick_map, returned, preferred_element_type=jnp.float32).reshape(
        top_count, tok_rows, width_part
    )
    mixed = jnp.sum(picked * jnp.transpose(route_weights)[:, :, None], axis=0)
    out_sum = lax.psum(jnp.sum(mixed * mixed, axis=1), "tp")
    out_scale = lax.rsqrt(out_sum / width_full + epsilon)
    return (mixed * out_scale[:, None] * post_gain[None, :]).astype(jnp.bfloat16)


def solution(mesh):
    return jax.shard_map(
        on_device,
        mesh=mesh,
        in_specs=(
            P("ep", "tp"),
            P("ep", None),
            P("ep", None),
            P("tp"),
            P("tp"),
            P("ep", None, "tp"),
            P("ep", None, "tp"),
            P("ep", None, "tp"),
        ),
        out_specs=P("ep", "tp"),
        check_vma=False,
    )
```

profile of v0, /device:TPU:0, one launch (start us, length us, event | category | flops | bytes accessed | tf_op | source)
XLA Modules:
  0.0 170.0 jit_solution(17323781832735627482)
XLA Ops:
  6.5 0.0 all-gather.4.cloned.1.call-start
  6.5 0.8 copy.39
  7.4 0.1 eq.65
  7.5 0.1 eq.61
  7.7 1.1 reduce-window.6
  8.8 0.2 slice_reduce_fusion
  9.1 0.1 fusion.34
  9.2 0.1 reduce_sum.51
  9.3 0.1 copy.41
  9.4 0.7 add_bitcast_fusion
  10.1 0.2 fusion.24
  10.3 1.1 fusion.28
  11.4 8.4 %psum.14 = f32[256]{0:T(256)S(1)} all-reduce(f32[256]{0:T(256)S(1)} %fusion.28), channel_id=1, replica_groups=mesh['ep'=8,'tp'=4] {'tp'}, use_global_device_ids=true, to_apply=%region_5.6 | all-reduce | flops 256 | bytes 2048 | tf_op jit(solution)/shard_map/psum | solution.py:21
  19.7 1.4 convolution_convert_fusion
  21.1 22.2 %all_to_all.8 = bf16[8,1,80,512]{3,2,1,0:T(8,128)(2,1)} all-to-all(bf16[8,1,80,512]{3,2,1,0:T(8,128)(2,1)S(1)} %bitcast.53), channel_id=1, replica_groups=mesh['ep'=8,'tp'=4] {'ep'}, dimensions={0} | all-to-all | bytes 1310720 | tf_op jit(solution)/shard_map/all_to_all | solution.py:39
  43.3 0.0 all-gather.4.cloned.1.call-update
  43.4 0.0 all-gather.6.cloned.1.call-start
  43.4 24.3 %all-gather.4.cloned.1.call-done = bf16[1,640,2048]{2,1,0:T(8,128)(2,1)} async-done(((bf16[1,640,512]{2,1,0:T(8,128)(2,1)}), bf16[1,640,2048]{2,1,0:T(8,128)(2,1)}) %all-gather.4.cloned.1.call-update) | async-done | bytes 2621456 | tf_op jit(solution)/shard_map/all_gather | solution.py:42
  67.8 0.0 copy-start.1
  67.8 0.0 copy-start.2
  67.8 5.6 %fusion.4 = f32[640,1024]{1,0:T(8,128)S(1)} fusion(bf16[1,2048,1024]{2,1,0:T(8,128)(2,1)} %param.13, bf16[1,640,2048]{2,1,0:T(8,128)(2,1)} %all-gather.4.cloned.1.call-done), kind=kOutput, calls=%fused_computation.4 | convolution fusion | flops 2684354560 | bytes 9437184 | tf_op jit(solution)/shard_map/erd,edh->erh/dot_general | solution.py:43
  73.4 0.0 copy-done.1
  73.4 0.0 copy-done.2
  73.4 4.2 %multiply_convert_fusion = bf16[640,1024]{1,0:T(8,128)(2,1)} fusion(f32[640,1024]{1,0:T(8,128)S(1)} %fusion.4, bf16[1,2048,1024]{2,1,0:T(8,128)(2,1)S(1)} %copy-done.1, bf16[1,640,2048]{2,1,0:T(8,128)(2,1)S(1)} %copy-done.2), kind=kOutput, calls=%fused_computation.8 | convolution fusion | flops 2688286720 | bytes 10747904 | tf_op jit(solution)/shard_map/erd,edh->erh/dot_general | solution.py:44
  77.6 0.0 all-gather.6.cloned.1.call-update
  77.6 40.6 %all-gather.6.cloned.1.call-done = bf16[640,4096]{1,0:T(8,128)(2,1)} async-done(((bf16[640,1024]{1,0:T(8,128)(2,1)}), bf16[640,4096]{1,0:T(8,128)(2,1)}) %all-gather.6.cloned.1.call-update) | async-done | bytes 5242896 | tf_op jit(solution)/shard_map/all_gather | solution.py:46
  118.2 6.6 %fusion.21 = bf16[1,1,640,512]{3,2,1,0:T(8,128)(2,1)S(1)} fusion(bf16[640,4096]{1,0:T(8,128)(2,1)} %all-gather.6.cloned.1.call-done, bf16[1,4096,512]{2,1,0:T(8,128)(2,1)} %param.15), kind=kOutput, calls=%fused_computation.17 | convolution fusion | flops 2684682240 | bytes 10092544 | tf_op jit(solution)/shard_map/erh,ehd->erd/dot_general | solution.py:47
  124.8 1.0 copy.50
  125.8 0.5 broadcast.77
  126.3 4.8 %reduce.3 = bf16[640,512]{1,0:T(8,128)(2,1)S(1)} reduce(bf16[640,1,1,512]{3,2,1,0:T(2,128)(2,1)S(1)} %bitcast.51, bf16[]{:T(256)} %broadcast.77), dimensions={1,2}, to_apply=%bitcast.50.reduce_sub_computation | reduce | bytes 1310722
  131.1 0.0 copy-start.3
  131.1 0.5 reshape.125
  131.6 23.4 %all_to_all.9 = bf16[8,2,20480]{2,1,0:T(2,128)(2,1)S(1)} all-to-all(bf16[8,2,20480]{2,1,0:T(2,128)(2,1)S(1)} %reshape.125), channel_id=1, replica_groups=mesh['ep'=8,'tp'=4] {'ep'}, dimensions={0} | all-to-all | bytes 1310720 | tf_op jit(solution)/shard_map/all_to_all | solution.py:51
  155.0 0.0 copy-start
  155.0 0.6 reshape.126
  155.6 0.0 copy-done.3
  155.6 0.6 fusion.18
  156.3 0.1 multiply_reduce_fusion
  156.4 6.0 %psum.15 = f32[256]{0:T(256)S(1)} all-reduce(f32[256]{0:T(256)S(1)} %multiply_reduce_fusion), channel_id=1, replica_groups=mesh['ep'=8,'tp'=4] {'tp'}, use_global_device_ids=true, to_apply=%region_8.9 | all-reduce | flops 256 | bytes 2048 | tf_op jit(solution)/shard_map/psum | solution.py:57
  162.4 0.0 copy-done
  162.4 0.8 multiply_convert_fusion.1
  (5 shorter events, 0.1 us)
Async XLA Ops:
  6.5 61.2 %all-gather.4.cloned.1.call-start = ((), (), s32[]{:S(2)}) async-start(), calls=%async_computation.2 | async-start | bytes 3276800 | tf_op jit(solution)/shard_map/all_gather | solution.py:42
  43.4 74.8 %all-gather.6.cloned.1.call-start = ((), (), s32[]{:S(2)}) async-start(), calls=%async_computation.3 | async-start | bytes 6553600 | tf_op jit(solution)/shard_map/all_gather | solution.py:46
  67.8 5.6 %copy-start.1 = (bf16[1,2048,1024]{2,1,0:T(8,128)(2,1)S(1)}, bf16[1,2048,1024]{2,1,0:T(8,128)(2,1)}, u32[]{:S(2)}) copy-start(bf16[1,2048,1024]{2,1,0:T(8,128)(2,1)} %param.14) | copy-start | bytes 12582916
  67.8 5.6 %copy-start.2 = (bf16[1,640,2048]{2,1,0:T(8,128)(2,1)S(1)}, bf16[1,640,2048]{2,1,0:T(8,128)(2,1)}, u32[]{:S(2)}) copy-start(bf16[1,640,2048]{2,1,0:T(8,128)(2,1)} %all-gather.4.cloned.1.call-done) | copy-start | bytes 7864324
  131.1 24.5 %copy-start.3 = (f32[256,2]{0,1:T(2,128)S(1)}, f32[256,2]{0,1:T(2,128)}, u32[]{:S(2)}) copy-start(f32[256,2]{0,1:T(2,128)} %param.10) | copy-start | bytes 6148
  155.0 7.4 %copy-start = (f32[512]{0:T(512)S(1)}, f32[512]{0:T(512)}, u32[]{:S(2)}) copy-start(f32[512]{0:T(512)} %param.12) | copy-start | bytes 6148
Sparse Core Ops, SparseCore 0:
  43.5 24.2 all-gather.3
  77.7 40.3 all-gather.5
where the time goes:
time: 170 us
  waiting for transfers between devices  64.9 us (38%)
  blocking collectives  59.9 us (35%)
  matrix products  18.4 us (11%)
  between operations  13.5 us (8%)
  other arithmetic  8.99 us (5%)
  local copies, waits for them, and re-layouts  4.19 us (2%)
    all_gather x1, waiting for transfers between devices, on_device(): hidden_whole = lax.all_gather(hidden, 'tp', axis=2, tiled=True)  40.6 us
    all_gather x1, waiting for transfers between devices, on_device(): features = lax.all_gather(arrived, 'tp', axis=2, tiled=True)  24.3 us
    all_to_all x1, blocking collectives, on_device(): lax.all_to_all(expert_out, 'ep', split_axis=2, concat_axis=0, tiled=True)  23.4 us
    all_to_all x1, blocking collectives, on_device(): lax.all_to_all(outgoing, 'ep', split_axis=0, concat_axis=2, tiled=True)  22.2 us
    psum x1, blocking collectives, on_device(): square_sum = lax.psum(jnp.sum(tok_float * tok_float, axis=1), 'tp')  8.37 us
    dot_general x1, matrix products, on_device(): jnp.einsum('erh,ehd->erd', hidden_whole, down_weight, preferred_element_t...  6.62 us
    psum x1, blocking collectives, on_device(): out_sum = lax.psum(jnp.sum(mixed * mixed, axis=1), 'tp')  5.95 us
    dot_general x1, matrix products, on_device(): jnp.einsum('erd,edh->erh', features, gate_weight, preferred_element_type=...  5.58 us
  transfers between devices with their start and end apart: 2, of which 2 were waited for; matrix products, arithmetic and copies ran while one was open for 0% of the time, Pallas kernels for 0%

commit v1 on v0

--- a/solution.py
+++ b/solution.py
@@ -48,7 +48,10 @@
         "erh,ehd->erd", hidden_whole, down_weight, preferred_element_type=jnp.float32
     )
     expert_out = result.astype(jnp.bfloat16).reshape(1, local_count, row_total, width_part)
-    returned = lax.all_to_all(expert_out, "ep", split_axis=2, concat_axis=0, tiled=True)
+    returned = jnp.concatenate(
+        lax.all_to_all(jnp.stack(jnp.split(expert_out, lax.axis_size("ep"), axis=2)), "ep", 0, 0),
+        axis=0,
+    )
     returned = returned.reshape(slot_total, width_part)
     picked = jnp.dot(pick_map, returned, preferred_element_type=jnp.float32).reshape(
         top_count, tok_rows, width_part

time: 170 us -> 163 us (0.959)
  other arithmetic: 8.99 us -> 4.19 us
  local copies, waits for them, and re-layouts: 4.19 us -> 1.61 us
    unnamed x1 -> x0, other arithmetic: 4.79 us -> none
where the time goes in v1:
time: 163 us
  waiting for transfers between devices  64.9 us (40%)
  blocking collectives  59.9 us (37%)
  matrix products  18.4 us (11%)
  between operations  13.6 us (8%)
  other arithmetic  4.19 us (3%)
    all_gather x1, waiting for transfers between devices, on_device(): hidden_whole = lax.all_gather(hidden, 'tp', axis=2, tiled=True)  40.6 us
    all_gather x1, waiting for transfers between devices, on_device(): features = lax.all_gather(arrived, 'tp', axis=2, tiled=True)  24.3 us
    all_to_all x1, blocking collectives, on_device(): lax.all_to_all(jnp.stack(jnp.split(expert_out, lax.axis_size('ep'), axis=...  23.4 us
    all_to_all x1, blocking collectives, on_device(): lax.all_to_all(outgoing, 'ep', split_axis=0, concat_axis=2, tiled=True)  22.2 us
    psum x1, blocking collectives, on_device(): square_sum = lax.psum(jnp.sum(tok_float * tok_float, axis=1), 'tp')  8.37 us
    dot_general x1, matrix products, on_device(): jnp.einsum('erh,ehd->erd', hidden_whole, down_weight, preferred_element_t...  6.62 us
    psum x1, blocking collectives, on_device(): out_sum = lax.psum(jnp.sum(mixed * mixed, axis=1), 'tp')  5.95 us
    dot_general x1, matrix products, on_device(): jnp.einsum('erd,edh->erh', features, gate_weight, preferred_element_type=...  5.58 us
  transfers between devices with their start and end apart: 2, of which 2 were waited for; matrix products, arithmetic and copies ran while one was open for 0% of the time, Pallas kernels for 0%

profile of v1, /device:TPU:0, one launch (start us, length us, event | category | flops | bytes accessed | tf_op | source)
XLA Modules:
  0.0 162.7 jit_solution(2785877836308564739)
XLA Ops:
  6.5 0.0 all-gather.4.cloned.1.call-start
  6.5 0.8 copy.29
  7.4 0.1 eq.65
  7.5 0.1 eq.61
  7.6 1.1 fusion.26
  8.7 8.4 %psum.14 = f32[256]{0:T(256)S(1)} all-reduce(f32[256]{0:T(256)S(1)} %fusion.26), channel_id=1, replica_groups=mesh['ep'=8,'tp'=4] {'tp'}, use_global_device_ids=true, to_apply=%region_5.6 | all-reduce | flops 256 | bytes 2048 | tf_op jit(solution)/shard_map/psum | solution.py:21
  17.1 1.1 reduce-window.6
  18.3 0.2 slice_reduce_fusion
  18.5 0.1 fusion.40
  18.6 0.1 reduce_sum.51
  18.8 0.1 copy.31
  18.8 0.7 add_bitcast_fusion
  19.5 0.2 fusion.24
  19.7 1.4 convolution_convert_fusion
  21.1 22.2 %all_to_all.14 = bf16[8,1,80,512]{3,2,1,0:T(8,128)(2,1)} all-to-all(bf16[8,1,80,512]{3,2,1,0:T(8,128)(2,1)S(1)} %bitcast.81), channel_id=1, replica_groups=mesh['ep'=8,'tp'=4] {'ep'}, dimensions={0} | all-to-all | bytes 1310720 | tf_op jit(solution)/shard_map/all_to_all | solution.py:39
  43.3 0.0 all-gather.4.cloned.1.call-update
  43.3 0.0 all-gather.6.cloned.1.call-start
  43.4 24.3 %all-gather.4.cloned.1.call-done = bf16[1,640,2048]{2,1,0:T(8,128)(2,1)} async-done(((bf16[1,640,512]{2,1,0:T(8,128)(2,1)}), bf16[1,640,2048]{2,1,0:T(8,128)(2,1)}) %all-gather.4.cloned.1.call-update) | async-done | bytes 2621456 | tf_op jit(solution)/shard_map/all_gather | solution.py:42
  67.7 0.0 copy-start.1
  67.7 0.0 copy-start.2
  67.7 5.6 %fusion.4 = f32[640,1024]{1,0:T(8,128)S(1)} fusion(bf16[1,2048,1024]{2,1,0:T(8,128)(2,1)} %param.13, bf16[1,640,2048]{2,1,0:T(8,128)(2,1)} %all-gather.4.cloned.1.call-done), kind=kOutput, calls=%fused_computation.4 | convolution fusion | flops 2684354560 | bytes 9437184 | tf_op jit(solution)/shard_map/erd,edh->erh/dot_general | solution.py:43
  73.3 0.0 copy-done.1
  73.4 0.0 copy-done.2
  73.4 4.2 %multiply_convert_fusion = bf16[640,1024]{1,0:T(8,128)(2,1)} fusion(f32[640,1024]{1,0:T(8,128)S(1)} %fusion.4, bf16[1,2048,1024]{2,1,0:T(8,128)(2,1)S(1)} %copy-done.1, bf16[1,640,2048]{2,1,0:T(8,128)(2,1)S(1)} %copy-done.2), kind=kOutput, calls=%fused_computation.8 | convolution fusion | flops 2688286720 | bytes 10747904 | tf_op jit(solution)/shard_map/erd,edh->erh/dot_general | solution.py:44
  77.6 0.0 all-gather.6.cloned.1.call-update
  77.6 40.6 %all-gather.6.cloned.1.call-done = bf16[640,4096]{1,0:T(8,128)(2,1)} async-done(((bf16[640,1024]{1,0:T(8,128)(2,1)}), bf16[640,4096]{1,0:T(8,128)(2,1)}) %all-gather.6.cloned.1.call-update) | async-done | bytes 5242896 | tf_op jit(solution)/shard_map/all_gather | solution.py:46
  118.1 6.6 %fusion.21 = bf16[1,1,640,512]{3,2,1,0:T(8,128)(2,1)S(1)} fusion(bf16[640,4096]{1,0:T(8,128)(2,1)} %all-gather.6.cloned.1.call-done, bf16[1,4096,512]{2,1,0:T(8,128)(2,1)} %param.15), kind=kOutput, calls=%fused_computation.17 | convolution fusion | flops 2684682240 | bytes 10092544 | tf_op jit(solution)/shard_map/erh,ehd->erd/dot_general | solution.py:47
  124.8 0.0 copy-start.3
  124.8 0.0 copy-start
  124.9 23.4 %all_to_all.15 = bf16[8,1,1,80,512]{4,3,2,1,0:T(8,128)(2,1)S(1)} all-to-all(bf16[8,1,1,80,512]{4,3,2,1,0:T(8,128)(2,1)S(1)} %fusion.32), channel_id=1, replica_groups=mesh['ep'=8,'tp'=4] {'ep'}, dimensions={0} | all-to-all | bytes 1310720 | tf_op jit(solution)/shard_map/all_to_all | solution.py:52
  148.3 0.0 copy-done.3
  148.3 0.6 fusion.18
  148.9 0.1 multiply_reduce_fusion
  149.1 6.0 %psum.15 = f32[256]{0:T(256)S(1)} all-reduce(f32[256]{0:T(256)S(1)} %multiply_reduce_fusion), channel_id=1, replica_groups=mesh['ep'=8,'tp'=4] {'tp'}, use_global_device_ids=true, to_apply=%region_8.9 | all-reduce | flops 256 | bytes 2048 | tf_op jit(solution)/shard_map/psum | solution.py:60
  155.0 0.0 copy-done
  155.0 0.8 multiply_convert_fusion.1
  (13 shorter events, 0.1 us)
Async XLA Ops:
  6.5 61.2 %all-gather.4.cloned.1.call-start = ((), (), s32[]{:S(2)}) async-start(), calls=%async_computation.2 | async-start | bytes 3276800 | tf_op jit(solution)/shard_map/all_gather | solution.py:42
  43.3 74.8 %all-gather.6.cloned.1.call-start = ((), (), s32[]{:S(2)}) async-start(), calls=%async_computation.3 | async-start | bytes 6553600 | tf_op jit(solution)/shard_map/all_gather | solution.py:46
  67.7 5.6 %copy-start.1 = (bf16[1,2048,1024]{2,1,0:T(8,128)(2,1)S(1)}, bf16[1,2048,1024]{2,1,0:T(8,128)(2,1)}, u32[]{:S(2)}) copy-start(bf16[1,2048,1024]{2,1,0:T(8,128)(2,1)} %param.14) | copy-start | bytes 12582916
  67.7 5.6 %copy-start.2 = (bf16[1,640,2048]{2,1,0:T(8,128)(2,1)S(1)}, bf16[1,640,2048]{2,1,0:T(8,128)(2,1)}, u32[]{:S(2)}) copy-start(bf16[1,640,2048]{2,1,0:T(8,128)(2,1)} %all-gather.4.cloned.1.call-done) | copy-start | bytes 7864324
  124.8 23.5 %copy-start.3 = (f32[256,2]{0,1:T(2,128)S(1)}, f32[256,2]{0,1:T(2,128)}, u32[]{:S(2)}) copy-start(f32[256,2]{0,1:T(2,128)} %param.10) | copy-start | bytes 6148
  124.8 30.2 %copy-start = (f32[512]{0:T(512)S(1)}, f32[512]{0:T(512)}, u32[]{:S(2)}) copy-start(f32[512]{0:T(512)} %param.12) | copy-start | bytes 6148
Sparse Core Ops, SparseCore 0:
  43.5 24.2 all-gather.3
  77.7 40.3 all-gather.5
